TPU v7x, 32 devices: a whole 2x2x4 slice. The times are simulated.
32 devices in a mesh: vp: 8 (over z, x), dp: 4 (over y, core).
Axes of the slice: x: 2, y: 2, z: 4, core: 2. Of those that a mesh axis runs over, the one named last changes fastest.
Arguments:
- hidden_rows: bfloat16 [768, 4, 2048], P('vp', 'dp'), may hold values from -48 to 48
- norm_gain: float32 [2048], replicated, may hold values from 0.1 to 1.9
- vocab_matrix: bfloat16 [2048, 8192], P(None, 'vp'), may hold values from -3 to 3
- vocab_bias: float32 [8192], P('vp'), may hold values from -4 to 4
- targets: int32 [768, 4], P(None, 'dp'), may hold values from 0 to 8191
- loss_weight: float32 [768, 4], P(None, 'dp'), may hold values from 0.5 to 8
Outputs:
- losses: float32 [768, 4], P('vp', 'dp')
- norm_grad: float32 [768, 4, 2048], P('vp', 'dp')
- vocab_grad: float32 [2048, 8192], P('dp', 'vp')
All inputs are finite; a program needn't handle non-finite values.
Results may differ from a plain program's by a relative error of at most 0.0056.
Values may be sent and summed in bfloat16 or wider, within the bound.
A program may use at most 64 MiB of HBM per device.

v0:
```python
import jax
import jax.numpy as jnp
from jax import lax
from jax.sharding import PartitionSpec as P

epsilon = 1e-06
penalty = 0.005


def merged(part, axis, combine):
    gathered = jax.tree.map(lambda a: lax.all_gather(a, axis), part)

    def take(source):
        return jax.tree.map(lambda a: lax.dynamic_index_in_dim(a, source, 0, False), gathered)

    return lax.fori_loop(
        1, lax.axis_size(axis), lambda source, state: combine(state, take(source)), take(0)
    )


def join_stats(left_stats, right_stats):
    maxima = jnp.maximum(left_stats[0], right_stats[0])
    totals = left_stats[1] * jnp.exp(left_stats[0] - maxima) + right_stats[1] * jnp.exp(
        right_stats[0] - maxima
    )
    return (maxima, totals, left_stats[2] + right_stats[2])


def local(hidden_rows, norm_gain, vocab_matrix, vocab_bias, targets, loss_weight):
    inputs = hidden_rows[:, 0, :].astype(jnp.float32)
    inverse_rms = lax.rsqrt(jnp.mean(inputs * inputs, axis=-1, keepdims=True) + epsilon)
    unit_rows = inputs * inverse_rms
    normed = (unit_rows * norm_gain).astype(jnp.bfloat16)
    rows_all = lax.all_gather(normed, "vp", axis=0, tiled=True)
    total_rows = rows_all.shape[0]
    columns = vocab_matrix.shape[1]
    target_col = targets[:, 0] - lax.axis_index("vp") * columns
    weights = loss_weight[:, 0]
    block_rows = min(768, total_rows)
    block_count = total_rows // block_rows
    column_ids = lax.broadcasted_iota(jnp.int32, (block_rows, columns), 1)
    block_ids = jnp.arange(block_count, dtype=jnp.int32)

    def block_target():
        return column_ids == target_col[:, None]

    def block_stats(scores):
        maxima = jnp.max(scores, axis=1)
        totals = jnp.sum(jnp.exp(scores - maxima[:, None]), axis=1)
        target_score = jnp.sum(jnp.where(block_target(), scores, 0.0), axis=1)
        return (maxima, totals, target_score)

    def first_pass(block_index):
        scores = (
            jnp.dot(rows_all, vocab_matrix, preferred_element_type=jnp.float32)
            + vocab_bias[None, :]
        )
        return (scores,) + block_stats(scores)

    kept, maxima, totals, target_score = lax.map(first_pass, block_ids)
    maxima, totals, target_score = merged(
        (maxima.reshape(total_rows), totals.reshape(total_rows), target_score.reshape(total_rows)),
        "vp",
        join_stats,
    )
    log_total = maxima + jnp.log(totals)
    loss_all = log_total - target_score + penalty * log_total * log_total

    def block_grads(scores):
        probs = jnp.exp(scores - log_total[:, None])
        return (
            weights[:, None]
            * (
                (1.0 + 2.0 * penalty * log_total)[:, None] * probs
                - jnp.where(block_target(), 1.0, 0.0)
            )
        ).astype(jnp.bfloat16)

    score_grad = lax.map(lambda pair: block_grads(pair[0]), (kept, block_ids))
    score_grad = score_grad.reshape(total_rows, columns)
    own_count = inputs.shape[0]
    row_grad = lax.psum_scatter(
        lax.dot_general(
            score_grad, vocab_matrix, (((1,), (1,)), ((), ())), preferred_element_type=jnp.float32
        ),
        "vp",
        scatter_dimension=0,
        tiled=True,
    )
    partial_grad = jnp.einsum("td,tv->dv", rows_all, score_grad, preferred_element_type=jnp.float32)
    vocab_grad = lax.psum_scatter(partial_grad, "dp", scatter_dimension=0, tiled=True)
    own_loss = lax.dynamic_slice_in_dim(loss_all, lax.axis_index("vp") * own_count, own_count, 0)
    scaled_grad = norm_gain * row_grad
    norm_grad = inverse_rms * (
        scaled_grad - unit_rows * jnp.mean(scaled_grad * unit_rows, axis=-1, keepdims=True)
    )
    return (own_loss[:, None], norm_grad[:, None, :], vocab_grad)


def solution(mesh):
    in_specs = (P("vp", "dp", None), P(), P(None, "vp"), P("vp"), P(None, "dp"), P(None, "dp"))
    out_specs = (P("vp", "dp"), P("vp", "dp", None), P("dp", "vp"))
    return jax.shard_map(local, mesh=mesh, in_specs=in_specs, out_specs=out_specs, check_vma=False)
```

profile of v0, /device:TPU:0, one launch (start us, length us, event | category | flops | bytes accessed | tf_op | source)
XLA Modules:
  0.0 378.8 jit_solution(17239342797568458852)
XLA Ops:
  7.2 0.0 all-gather.8.cloned.1.call-start
  7.2 1.2 fusion.8
  8.4 1.9 fusion.3
  10.3 0.0 all-gather.8.cloned.1.call-update
  10.3 0.0 reduce-scatter.3.cloned.1.call-start
  10.4 0.7 reduce.7
  11.1 0.7 subtract_reduce_fusion
  11.8 0.0 copy-start.2
  11.8 61.7 %all-gather.8.cloned.1.call-done = bf16[768,2048]{1,0:T(8,128)(2,1)} async-done(((bf16[96,2048]{1,0:T(8,128)(2,1)}), bf16[768,2048]{1,0:T(8,128)(2,1)}) %all-gather.8.cloned.1.call-update) | async-done | bytes 3145744 | tf_op jit(solution)/shard_map/all_gather | solution.py:34
  73.5 6.3 %add_reduce_fusion = (f32[768]{0:T(1024)S(1)}, f32[768,1024]{1,0:T(8,128)S(1)}) fusion(f32[1024]{0:T(1024)} %param.11, bf16[768,2048]{1,0:T(8,128)(2,1)} %all-gather.8.cloned.1.call-done, bf16[2048,1024]{1,0:T(8,128)(2,1)} %param.10), kind=kOutput, calls=%fused_computation.8 | convolution fusion | flops 3222797568 | bytes 10492928 | tf_op jit(solution)/shard_map/while/body/eval_jaxpr/dot_general | solution.py:55
  79.8 0.0 copy-done.2
  79.8 1.1 select_reduce_fusion
  81.0 30.5 %all-gather.4 = f32[8,1,768]{2,1,0:T(1,128)S(1)} all-gather(f32[1,1,768]{2,1,0:T(1,128)S(1)} %reshape.41), channel_id=3, replica_groups=mesh['vp'=8,'dp'=4] {'vp'}, dimensions={0}, use_global_device_ids=true | all-gather | bytes 27648 | tf_op jit(solution)/shard_map/all_gather | solution.py:11
  111.5 30.5 %all-gather.5 = f32[8,1,768]{2,1,0:T(1,128)S(1)} all-gather(f32[1,1,768]{2,1,0:T(1,128)S(1)} %reshape.43), channel_id=4, replica_groups=mesh['vp'=8,'dp'=4] {'vp'}, dimensions={0}, use_global_device_ids=true | all-gather | bytes 27648 | tf_op jit(solution)/shard_map/all_gather | solution.py:11
  142.1 30.5 %all-gather.3 = f32[8,1,768]{2,1,0:T(1,128)S(1)} all-gather(f32[1,1,768]{2,1,0:T(1,128)S(1)} %reshape.39), channel_id=2, replica_groups=mesh['vp'=8,'dp'=4] {'vp'}, dimensions={0}, use_global_device_ids=true | all-gather | bytes 27648 | tf_op jit(solution)/shard_map/all_gather | solution.py:11
  172.7 0.8 while.12
  173.5 8.4 %fusion.11 = f32[768,2048]{1,0:T(8,128)} fusion(bf16[2048,1024]{1,0:T(8,128)(2,1)} %param.10, f32[768,1024]{1,0:T(8,128)S(1)} %get-tuple-element.264, f32[768]{0:T(1024)S(1)} %get-tuple-element.260, f32[768]{0:T(1024)S(1)} %get-tuple-element.259, f32[768]{0:T(1024)S(1)} %reduce.7, s32[768]{0:T(1024)S(1)} %subtract_reduce_fusion, f32[1024]{0:T(1024)S(1)} %copy-done.2), kind=kOutput, calls=%fused_computation.35 | convolution fusion | flops 3227516928 | bytes 13647872 | tf_op jit(solution)/shard_map/dot_general | solution.py:83
  181.9 0.0 reduce-scatter.3.cloned.1.call-update
  181.9 0.0 reduce-scatter.5.cloned.1.call-start
  181.9 9.2 %fusion.10 = f32[2048,1024]{1,0:T(8,128)} fusion(bf16[768,2048]{1,0:T(8,128)(2,1)} %all-gather.8.cloned.1.call-done, f32[768,1024]{1,0:T(8,128)S(1)} %get-tuple-element.264, f32[768]{0:T(1024)S(1)} %get-tuple-element.260, f32[768]{0:T(1024)S(1)} %get-tuple-element.259, f32[768]{0:T(1024)S(1)} %reduce.7, s32[768]{0:T(1024)S(1)} %subtract_reduce_fusion, ...), kind=kOutput, calls=%fused_computation.34 | convolution fusion | flops 3227516928 | bytes 14696448 | tf_op jit(solution)/shard_map/td,tv->dv/dot_general | solution.py:90
  191.1 0.0 copy-start
  191.1 0.0 copy-start.1
  191.1 0.0 reduce-scatter.5.cloned.1.call-update
  191.1 0.6 dynamic-slice_bitcast_fusion
  191.7 106.7 %reduce-scatter.3.cloned.1.call-done = f32[96,2048]{1,0:T(8,128)} async-done(((f32[768,2048]{1,0:T(8,128)}), f32[96,2048]{1,0:T(8,128)}) %reduce-scatter.3.cloned.1.call-update) | async-done | bytes 786448 | tf_op jit(solution)/shard_map/reduce_scatter | solution.py:82
  298.4 0.0 copy-done
  298.5 0.0 copy-done.1
  298.5 1.4 fusion.4
  299.9 1.4 fusion.7
  301.3 1.7 copy.10
  303.0 69.3 %reduce-scatter.5.cloned.1.call-done = f32[512,1024]{1,0:T(8,128)} async-done(((f32[2048,1024]{1,0:T(8,128)}), f32[512,1024]{1,0:T(8,128)}) %reduce-scatter.5.cloned.1.call-update) | async-done | bytes 2097168 | tf_op jit(solution)/shard_map/reduce_scatter | solution.py:91
  (41 shorter events, 0.5 us)
Async XLA Ops:
  7.2 66.3 %all-gather.8.cloned.1.call-start = ((), (), s32[]{:S(2)}) async-start(), calls=%async_computation.2 | async-start | bytes 3538944 | tf_op jit(solution)/shard_map/all_gather | solution.py:34
  10.3 288.1 %reduce-scatter.3.cloned.1.call-start = ((), (), s32[]{:S(2)}) async-start(), calls=%async_computation.3 | async-start | bytes 7077888 | tf_op jit(solution)/shard_map/reduce_scatter | solution.py:82
  11.8 68.0 %copy-start.2 = (f32[1024]{0:T(1024)S(1)}, f32[1024]{0:T(1024)}, u32[]{:S(2)}) copy-start(f32[1024]{0:T(1024)} %param.11) | copy-start | bytes 12292
  181.9 190.4 %reduce-scatter.5.cloned.1.call-start = ((), (), s32[]{:S(2)}) async-start(), calls=%async_computation.4 | async-start | bytes 10485760 | tf_op jit(solution)/shard_map/reduce_scatter | solution.py:91
  191.1 107.4 %copy-start = (bf16[96,1,2048]{2,0,1:T(8,128)(2,1)S(1)}, bf16[96,1,2048]{2,0,1:T(8,128)(2,1)}, u32[]{:S(2)}) copy-start(bf16[96,1,2048]{2,0,1:T(8,128)(2,1)} %param.8) | copy-start | bytes 1179652
  191.1 107.4 %copy-start.1 = (f32[2048]{0:T(1024)S(1)}, f32[2048]{0:T(1024)}, u32[]{:S(2)}) copy-start(f32[2048]{0:T(1024)} %param.9) | copy-start | bytes 24580
Sparse Core Ops, SparseCore 0:
  10.7 62.7 all-gather.7
  182.0 116.4 reduce-scatter.2
  301.6 70.6 reduce-scatter.4
where the time goes:
time: 379 us
  waiting for transfers between devices  238 us (63%)
  blocking collectives  91.6 us (24%)
  matrix products  23.9 us (6%)
  between operations  13.9 us (4%)
  other arithmetic  8.56 us (2%)
    reduce_scatter x1, waiting for transfers between devices, local(): lax.psum_scatter(lax.dot_general(score_grad, vocab_matrix, (((1,), (1,)),...  107 us
    all_gather x3, blocking collectives, merged(): gathered = jax.tree.map(lambda a: lax.all_gather(a, axis), part)  91.6 us
    reduce_scatter x1, waiting for transfers between devices, local(): lax.psum_scatter(partial_grad, 'dp', scatter_dimension=0, tiled=True)  69.3 us
    all_gather x1, waiting for transfers between devices, local(): rows_all = lax.all_gather(normed, 'vp', axis=0, tiled=True)  61.7 us
    dot_general x1, matrix products, local(): jnp.einsum('td,tv->dv', rows_all, score_grad, preferred_element_type=jnp....  9.17 us
    dot_general x1, matrix products, local(): lax.dot_general(score_grad, vocab_matrix, (((1,), (1,)), ((), ())), prefe...  8.4 us
  transfers between devices with their start and end apart: 3, of which 3 were waited for; matrix products, arithmetic and copies ran while one was open for 4% of the time, Pallas kernels for 0%

commit v1 on v0

v1 whole, which is shorter than its diff:
```python
import functools

import jax
import jax.numpy as jnp
from jax import lax
from jax.experimental import pallas as pl
from jax.experimental.pallas import tpu as pltpu
from jax.sharding import PartitionSpec as P

epsilon = 1e-06
penalty = 0.005
MESH = pl.DeviceIdType.MESH
CHUNKS = 2


def kernel(
    n, nx, ny,
    hid_ref, gain_ref, mat_hbm, bias_ref, tgt_ref, wgt_ref,
    loss_ref, ngrad_ref, vout_ref,
    rows, mat, scores, sg, part, xsend, xrecv, zsend, zrecv,
    rowst, csend, crecv, ysend, yrecv, own, statc, stats_out, stats_all, colv,
    mat_sem, ag_r, ag_up, ag_dn, ag_x, st_s, st_r, xs, xr, zs, zr, cs, cr, ys, yr,
):
    nz = n // nx
    me = lax.axis_index("vp")
    dme = lax.axis_index("dp")
    z, x = me // nx, me % nx
    y, core = dme // 2, dme % 2
    own_rows, width = hid_ref.shape
    columns = mat.shape[1]
    total = n * own_rows
    half = width // CHUNKS
    out_rows = vout_ref.shape[0]
    f32, bf16 = jnp.float32, jnp.bfloat16

    mat_copy = pltpu.make_async_copy(mat_hbm, mat, mat_sem)
    mat_copy.start()

    barrier = pltpu.get_barrier_semaphore()

    def greet(k, _):
        pl.semaphore_signal(barrier, inc=1, device_id={"vp": (me + k) % n}, device_id_type=MESH)
        return 0

    lax.fori_loop(1, n, greet, 0)
    partner = y * 2 + 1 - core
    pl.semaphore_signal(barrier, inc=1, device_id={"dp": partner}, device_id_type=MESH)
    for q in range(ny - 1):
        pl.semaphore_signal(
            barrier, inc=1, device_id={"dp": ((y + 1 + q) % ny) * 2 + core}, device_id_type=MESH
        )

    hid = hid_ref[...].astype(f32)
    inverse_rms = lax.rsqrt(jnp.mean(hid * hid, axis=-1, keepdims=True) + epsilon)
    rows[me] = (hid * inverse_rms * gain_ref[...]).astype(bf16)
    pl.semaphore_wait(barrier, n - 1 + ny)

    def ag_copy(b, h, send_sem, target):
        piece = rows.at[b, :, pl.ds(h * half, half)]
        return pltpu.make_async_remote_copy(
            src_ref=piece, dst_ref=piece, send_sem=send_sem, recv_sem=ag_r.at[b * CHUNKS + h],
            device_id={"vp": target}, device_id_type=MESH,
        )

    def up_copy(zz, h):
        return ag_copy(zz * nx + x, h, ag_up.at[zz * CHUNKS + h], (z + 1) * nx + x)

    def down_copy(zz, h):
        return ag_copy(zz * nx + x, h, ag_dn.at[zz * CHUNKS + h], (z - 1) * nx + x)

    def x_copy(zz, h, j):
        return ag_copy(
            zz * nx + x, h, ag_x.at[((j - 1) * nz + zz) * CHUNKS + h], z * nx + (x + j) % nx
        )

    def got(b, h):
        ag_copy(b, h, ag_up.at[0], (me + 1) % n).wait_recv()

    def forward(k, h):
        below, above = z - k, z + k

        @pl.when(below >= 0)
        def _():
            @pl.when(k > 0)
            def _():
                got(below * nx + x, h)

            @pl.when(z < nz - 1)
            def _():
                up_copy(below, h).start()

            @pl.when((k == 0) & (z > 0))
            def _():
                down_copy(below, h).start()

            for j in range(1, nx):
                x_copy(below, h, j).start()

        @pl.when((k > 0) & (above < nz))
        def _():
            got(above * nx + x, h)

            @pl.when(z > 0)
            def _():
                down_copy(above, h).start()

            for j in range(1, nx):
                x_copy(above, h, j).start()

    lanes = lax.broadcasted_iota(jnp.int32, (own_rows, 128), 1)
    column_ids = lax.broadcasted_iota(jnp.int32, (own_rows, columns), 1)

    def score(b):
        s = jnp.dot(rows[b], mat[...], preferred_element_type=f32) + bias_ref[...]
        scores[b] = s
        m = jnp.max(s, axis=1, keepdims=True)
        t = jnp.sum(jnp.exp(s - m), axis=1, keepdims=True)
        hit = column_ids == tgt_ref[b] - me * columns
        g = jnp.sum(jnp.where(hit, s, 0.0), axis=1, keepdims=True)
        statc[b] = jnp.where(lanes == 0, m, jnp.where(lanes == 1, t, g))

    def gather_step(k, _):
        @pl.when(k < nz)
        def _():
            for h in range(CHUNKS):
                forward(k, h)

        @pl.when(k == 0)
        def _():
            mat_copy.wait()

        def visit(t, _):
            i, j = t % 2, t // 2
            kk = jnp.where(j == 0, k, k - 1)
            zz = z + (2 * i - 1) * kk
            b = zz * nx + (x + j) % nx

            @pl.when((kk >= 0) & (zz >= 0) & (zz < nz) & ((kk > 0) | (i == 0)))
            def _():
                @pl.when(j > 0)
                def _():
                    for h in range(CHUNKS):
                        got(b, h)

                score(b)

            return 0

        lax.fori_loop(0, 2 * nx, visit, 0)
        return 0

    lax.fori_loop(0, nz + 1, gather_step, 0)

    packed = jnp.transpose(statc[...].reshape(total, 128))[0:8]
    stats_out[...] = packed
    stats_all[0] = packed

    def stat_copy(k):
        return pltpu.make_async_remote_copy(
            src_ref=stats_out, dst_ref=stats_all.at[k], send_sem=st_s.at[k], recv_sem=st_r.at[k],
            device_id={"vp": (me + k) % n}, device_id_type=MESH,
        )

    def stat_start(k, _):
        stat_copy(k).start()
        return 0

    lax.fori_loop(1, n, stat_start, 0)

    def turn(c, _):
        at = pl.ds(pl.multiple_of(c * 128, 128), 128)
        rowst[at, :] = jnp.transpose(rows[:, :, at].astype(f32).reshape(total, 128)).astype(bf16)
        return 0

    lax.fori_loop(0, width // 128, turn, 0)

    def stat_wait(k, _):
        stat_copy(k).wait()
        return 0

    lax.fori_loop(1, n, stat_wait, 0)
    every = stats_all[...]
    peak = jnp.max(every[:, 0:1, :], axis=0)
    summed = jnp.sum(every[:, 1:2, :] * jnp.exp(every[:, 0:1, :] - peak[None]), axis=0)
    hit_score = jnp.sum(every[:, 2:3, :], axis=0)
    log_total = peak + jnp.log(summed)
    loss = log_total - hit_score + penalty * log_total * log_total
    stacked = jnp.concatenate([log_total, loss, jnp.zeros((126, total), f32)], axis=0)
    colv[...] = jnp.transpose(stacked).reshape(n, own_rows, 128)
    loss_ref[...] = colv[me][:, 1:2]

    def grads(b, _):
        lt = colv[b][:, 0:1]
        w = wgt_ref[b]
        hit = column_ids == tgt_ref[b] - me * columns
        probs = jnp.exp(scores[b] - lt)
        sg[b] = (
            w * ((1.0 + 2.0 * penalty * lt) * probs - jnp.where(hit, 1.0, 0.0))
        ).astype(bf16)
        return 0

    lax.fori_loop(0, n, grads, 0)

    def x_send(slot, j):
        return pltpu.make_async_remote_copy(
            src_ref=xsend.at[slot], dst_ref=xrecv.at[slot], send_sem=xs.at[slot], recv_sem=xr.at[slot],
            device_id={"vp": z * nx + (x + j) % nx}, device_id_type=MESH,
        )

    def row_part(u, _):
        j = (u // (2 * nz) + 1) % nx
        k = nz - 1 - (u // 2) % nz
        i = u % 2
        zz = z + (2 * i - 1) * k

        @pl.when((zz >= 0) & (zz < nz) & ((k > 0) | (i == 0)))
        def _():
            b = zz * nx + (x + j) % nx
            p = lax.dot_general(sg[b], mat[...], (((1,), (1,)), ((), ())), preferred_element_type=f32)

            @pl.when(j > 0)
            def _():
                slot = (j - 1) * nz + zz
                xsend[slot] = p.astype(bf16)
                x_send(slot, j).start()

            @pl.when(j == 0)
            def _():
                part[zz] = p

        return 0

    def flat_grad():
        if own_rows % 16 == 0:
            return sg[...].reshape(total, columns)
        return sg[...].astype(f32).reshape(total, columns).astype(bf16)

    def vocab_part(d):
        at = pl.ds(pl.multiple_of(d * out_rows, out_rows), out_rows)
        return jnp.dot(rowst[at, :], flat_grad(), preferred_element_type=f32)

    def core_copy(q):
        return pltpu.make_async_remote_copy(
            src_ref=csend.at[q], dst_ref=crecv.at[q], send_sem=cs.at[q], recv_sem=cr.at[q],
            device_id={"dp": partner}, device_id_type=MESH,
        )

    def y_copy(q):
        return pltpu.make_async_remote_copy(
            src_ref=ysend.at[q], dst_ref=yrecv.at[q], send_sem=ys.at[q], recv_sem=yr.at[q],
            device_id={"dp": ((y + 1 + q) % ny) * 2 + core}, device_id_type=MESH,
        )

    def core_part(q, _):
        csend[q] = vocab_part(((y + 1 + q) % ny) * 2 + 1 - core).astype(bf16)
        core_copy(q).start()
        return 0

    def own_part(q, _):
        own[...] = vocab_part(((y + 1 + q) % ny) * 2 + core)
        core_copy(q).wait_recv()

        @pl.when(q < ny - 1)
        def _():
            slot = jnp.minimum(q, max(ny - 2, 0))
            ysend[slot] = (own[...] + crecv[q].astype(f32)).astype(bf16)
            y_copy(slot).start()

        @pl.when(q == ny - 1)
        def _():
            vout_ref[...] = own[...] + crecv[q].astype(f32)

        return 0

    def z_copy(i, zz):
        return pltpu.make_async_remote_copy(
            src_ref=zsend.at[zz], dst_ref=zrecv.at[i * nz + zz], send_sem=zs.at[zz],
            recv_sem=zr.at[i * nz + zz],
            device_id={"vp": (z + 2 * i - 1) * nx + x}, device_id_type=MESH,
        )

    def add_x(zz):
        for j in range(1, nx):
            slot = (j - 1) * nz + zz
            x_send(slot, j).wait_recv()
            part[zz] += xrecv[slot].astype(f32)

    def add_z(i, zz):
        z_copy(i, zz).wait_recv()
        part[zz] += zrecv[i * nz + zz].astype(f32)

    def chain(k):
        def one(i, _):
            zz = z + (2 * i - 1) * k

            @pl.when((zz >= 0) & (zz < nz))
            def _():
                add_x(zz)

                @pl.when(((i == 1) & (z > 0)) | ((i == 0) & (z < nz - 1)))
                def _():
                    add_z(i, zz)

                zsend[zz] = part[zz].astype(bf16)
                z_copy(i, zz).start()

            return 0

        lax.fori_loop(0, 2, one, 0)

    def chain_at(s, _):
        chain(nz - 1 - s)
        return 0

    lax.fori_loop(0, 2 * nz * (nx - 1), row_part, 0)
    lax.fori_loop(0, ny, core_part, 0)
    lax.fori_loop(2 * nz * (nx - 1), 2 * nz * nx, row_part, 0)
    lax.fori_loop(0, 1, chain_at, 0)
    lax.fori_loop(0, ny, own_part, 0)
    lax.fori_loop(1, nz - 1, chain_at, 0)

    add_x(z)

    @pl.when(z > 0)
    def _():
        add_z(1, z)

    @pl.when(z < nz - 1)
    def _():
        add_z(0, z)

    hid = hid_ref[...].astype(f32)
    inverse_rms = lax.rsqrt(jnp.mean(hid * hid, axis=-1, keepdims=True) + epsilon)
    unit = hid * inverse_rms
    scaled = gain_ref[...] * part[z]
    ngrad_ref[...] = inverse_rms * (scaled - unit * jnp.mean(scaled * unit, axis=-1, keepdims=True))

    for q in range(ny - 1):
        y_copy(q).wait_recv()
        vout_ref[...] += yrecv[q].astype(f32)

    def drain(zz, _):
        for h in range(CHUNKS):
            @pl.when((zz <= z) & (z < nz - 1))
            def _():
                up_copy(zz, h).wait_send()

            @pl.when((zz >= z) & (z > 0))
            def _():
                down_copy(zz, h).wait_send()

            for j in range(1, nx):
                x_copy(zz, h, j).wait_send()

        for j in range(1, nx):
            x_send((j - 1) * nz + zz, j).wait_send()

        @pl.when(zz > z)
        def _():
            z_copy(1, zz).wait_send()

        @pl.when(zz < z)
        def _():
            z_copy(0, zz).wait_send()

        return 0

    lax.fori_loop(0, nz, drain, 0)
    for q in range(ny):
        core_copy(q).wait_send()
    for q in range(ny - 1):
        y_copy(q).wait_send()


def solution(mesh):
    n, dp = mesh.shape["vp"], mesh.shape["dp"]
    ny = dp // 2
    nx = 1
    while (2 * nx) ** 2 <= n and n % (2 * nx) == 0:
        nx *= 2
    nz = n // nx

    def local(hidden_rows, norm_gain, vocab_matrix, vocab_bias, targets, loss_weight):
        own_rows, _, width = hidden_rows.shape
        columns = vocab_matrix.shape[1]
        total = n * own_rows
        out_rows = width // dp
        f32, bf16 = jnp.float32, jnp.bfloat16
        vmem = pl.BlockSpec(memory_space=pltpu.VMEM)
        dma = pltpu.SemaphoreType.DMA
        others = max(ny - 1, 1)
        xslots = max((nx - 1) * nz, 1)
        block = (own_rows, width)
        losses, norm_grad, vocab_grad = pl.pallas_call(
            functools.partial(kernel, n, nx, ny),
            out_shape=(
                jax.ShapeDtypeStruct((own_rows, 1), f32),
                jax.ShapeDtypeStruct(block, f32),
                jax.ShapeDtypeStruct((out_rows, columns), f32),
            ),
            in_specs=[vmem, vmem, pl.BlockSpec(memory_space=pl.ANY), vmem, vmem, vmem],
            out_specs=(vmem, vmem, vmem),
            scratch_shapes=[
                pltpu.VMEM((n,) + block, bf16),
                pltpu.VMEM((width, columns), bf16),
                pltpu.VMEM((n, own_rows, columns), f32),
                pltpu.VMEM((n, own_rows, columns), bf16),
                pltpu.VMEM((nz,) + block, f32),
                pltpu.VMEM((xslots,) + block, bf16),
                pltpu.VMEM((xslots,) + block, bf16),
                pltpu.VMEM((nz,) + block, bf16),
                pltpu.VMEM((2 * nz,) + block, bf16),
                pltpu.VMEM((width, total), bf16),
                pltpu.VMEM((ny, out_rows, columns), bf16),
                pltpu.VMEM((ny, out_rows, columns), bf16),
                pltpu.VMEM((others, out_rows, columns), bf16),
                pltpu.VMEM((others, out_rows, columns), bf16),
                pltpu.VMEM((out_rows, columns), f32),
                pltpu.VMEM((n, own_rows, 128), f32),
                pltpu.VMEM((8, total), f32),
                pltpu.VMEM((n, 8, total), f32),
                pltpu.VMEM((n, own_rows, 128), f32),
                dma,
                dma((n * CHUNKS,)),
                dma((nz * CHUNKS,)),
                dma((nz * CHUNKS,)),
                dma((xslots * CHUNKS,)),
                dma((n,)),
                dma((n,)),
                dma((xslots,)),
                dma((xslots,)),
                dma((nz,)),
                dma((2 * nz,)),
                dma((ny,)),
                dma((ny,)),
                dma((others,)),
                dma((others,)),
            ],
            compiler_params=pltpu.CompilerParams(
                collective_id=0, has_side_effects=True, vmem_limit_bytes=60 * 1024 * 1024
            ),
        )(
            hidden_rows.reshape(block),
            norm_gain.reshape(1, width),
            vocab_matrix,
            vocab_bias.reshape(1, columns),
            targets.reshape(n, own_rows, 1),
            loss_weight.reshape(n, own_rows, 1),
        )
        return losses, norm_grad.reshape(own_rows, 1, width), vocab_grad

    in_specs = (P("vp", "dp", None), P(), P(None, "vp"), P("vp"), P(None, "dp"), P(None, "dp"))
    out_specs = (P("vp", "dp"), P("vp", "dp", None), P("dp", "vp"))
    return jax.shard_map(local, mesh=mesh, in_specs=in_specs, out_specs=out_specs, check_vma=False)
```

time: 379 us -> 107 us (0.28)
  waiting for transfers between devices: 238 us -> 0 us
  Pallas kernels: 0 us -> 95 us
  blocking collectives: 91.6 us -> 0 us
  matrix products: 23.9 us -> 0 us
  between operations: 13.9 us -> 0.65 us
  other arithmetic: 8.56 us -> 1.4 us
  local copies, waits for them, and re-layouts: 2.7 us -> 9.39 us
    reduce_scatter x2 -> x0, waiting for transfers between devices: 176 us -> none  [the longest x1 107 us: local(): lax.psum_scatter(lax.dot_general(score_grad, vocab_matrix, (((1,), (1,)),...]
    pallas_call x0 -> x1, Pallas kernels: none -> 95 us  [local(): pl.pallas_call(functools.partial(kernel, n, nx, ny), out_shape=(jax.Shape...]
    all_gather x3 -> x0, blocking collectives: 91.6 us -> none  [merged(): gathered = jax.tree.map(lambda a: lax.all_gather(a, axis), part)]
    all_gather x1 -> x0, waiting for transfers between devices: 61.7 us -> none  [local(): rows_all = lax.all_gather(normed, 'vp', axis=0, tiled=True)]
    dot_general x3 -> x0, matrix products: 23.9 us -> none  [the longest x1 9.17 us: local(): jnp.einsum('td,tv->dv', rows_all, score_grad, preferred_element_type=jnp....]
    unnamed x13 -> x3, local copies, waits for them, and re-layouts: 1.73 us -> 7.36 us
  transfers between devices with their start and end apart: 3 -> 0, of which waited for: 3 -> 0; matrix products, arithmetic and copies ran while one was open for 4% -> 0% of each run, Pallas kernels for 0% -> 0%
where the time goes in v1:
time: 107 us; the launch traced here: 106 us
  Pallas kernels  95 us (89%)
  local copies, waits for them, and re-layouts  9.39 us (9%)
  other arithmetic  1.4 us (1%)
    pallas_call x1, Pallas kernels, local(): pl.pallas_call(functools.partial(kernel, n, nx, ny), out_shape=(jax.Shape...  95 us
    unnamed x3, local copies, waits for them, and re-layouts  7.36 us

profile of v1, /device:TPU:0, one launch (start us, length us, event | category | flops | bytes accessed | tf_op | source)
XLA Modules:
  0.0 106.4 jit_solution(16472433511255627660)
XLA Ops:
  0.6 0.7 reduce
  1.3 0.7 reduce.1
  2.0 1.0 reshape.31.wgt_ref
  3.1 1.0 reshape.30.tgt_ref
  4.1 95.0 %shard_map.85 = (f32[96,1]{1,0:T(8,128)}, f32[96,2048]{1,0:T(8,128)}, f32[512,1024]{1,0:T(8,128)}) custom-call(bf16[96,2048]{1,0:T(8,128)(2,1)} %bitcast.5, f32[1,2048]{1,0:T(1,128)} %bitcast.6, bf16[2048,1024]{1,0:T(8,128)(2,1)} %mat_hbm.1, f32[1,1024]{1,0:T(1,128)} %bitcast.7, s32[8,96,1]{2,1,0:T(8,128)} %reshape.30.tgt_ref, f32[8,96,1]{2,1,0:T(8,128)} %reshape.31.wgt_ref), custom_call_target="tpu_custom_call" | custom-call | tf_op jit(solution)/shard_map/pallas_call | solution.py:394
  99.1 1.4 %copy.13 = f32[96,1]{0,1:T(1,128)} copy(f32[96,1]{1,0:T(8,128)} %get-tuple-element.12) | data formatting | bytes 768
  100.5 2.8 %copy.14 = f32[96,1,2048]{2,1,0:T(1,128)} copy(f32[96,1,2048]{2,0,1:T(8,128)} %bitcast.4) | data formatting | bytes 1572864
  103.3 3.2 %copy.16 = f32[512,1024]{1,0:T(8,128)} copy(f32[512,1024]{1,0:T(8,128)} %get-tuple-element.20) | data formatting | bytes 4194304

commit v2 on v1

--- a/solution.py
+++ b/solution.py
@@ -18,7 +18,7 @@
     hid_ref, gain_ref, mat_hbm, bias_ref, tgt_ref, wgt_ref,
     loss_ref, ngrad_ref, vout_ref,
     rows, mat, scores, sg, part, xsend, xrecv, zsend, zrecv,
-    rowst, csend, crecv, ysend, yrecv, own, statc, stats_out, stats_all, colv,
+    rowst, csend, crecv, ysend, yrecv, own, statc, stats_out, stats_all, colv, tw,
     mat_sem, ag_r, ag_up, ag_dn, ag_x, st_s, st_r, xs, xr, zs, zr, cs, cr, ys, yr,
 ):
     nz = n // nx
@@ -53,6 +53,17 @@
     hid = hid_ref[...].astype(f32)
     inverse_rms = lax.rsqrt(jnp.mean(hid * hid, axis=-1, keepdims=True) + epsilon)
     rows[me] = (hid * inverse_rms * gain_ref[...]).astype(bf16)
+    turned = jnp.transpose(
+        jnp.concatenate(
+            [
+                (tgt_ref[...] - me * columns).astype(f32),
+                wgt_ref[...],
+                jnp.zeros((126, total), f32),
+            ],
+            axis=0,
+        )
+    )
+    tw[...] = turned.reshape(n, own_rows, 128)
     pl.semaphore_wait(barrier, n - 1 + ny)
 
     def ag_copy(b, h, send_sem, target):
@@ -108,14 +119,14 @@
                 x_copy(above, h, j).start()
 
     lanes = lax.broadcasted_iota(jnp.int32, (own_rows, 128), 1)
-    column_ids = lax.broadcasted_iota(jnp.int32, (own_rows, columns), 1)
+    column_ids = lax.broadcasted_iota(jnp.int32, (own_rows, columns), 1).astype(f32)
 
     def score(b):
         s = jnp.dot(rows[b], mat[...], preferred_element_type=f32) + bias_ref[...]
         scores[b] = s
         m = jnp.max(s, axis=1, keepdims=True)
         t = jnp.sum(jnp.exp(s - m), axis=1, keepdims=True)
-        hit = column_ids == tgt_ref[b] - me * columns
+        hit = column_ids == tw[b][:, 0:1]
         g = jnp.sum(jnp.where(hit, s, 0.0), axis=1, keepdims=True)
         statc[b] = jnp.where(lanes == 0, m, jnp.where(lanes == 1, t, g))
 
@@ -151,7 +162,11 @@
 
     lax.fori_loop(0, nz + 1, gather_step, 0)
 
-    packed = jnp.transpose(statc[...].reshape(total, 128))[0:8]
+    lined = jnp.transpose(statc[...].reshape(total, 128))
+    groups = total // 128
+    packed = jnp.concatenate(
+        [lined[s : s + 1, c * 128 : (c + 1) * 128] for s in range(3) for c in range(groups)], axis=0
+    )
     stats_out[...] = packed
     stats_all[0] = packed
 
@@ -180,30 +195,37 @@
 
     lax.fori_loop(1, n, stat_wait, 0)
     every = stats_all[...]
-    peak = jnp.max(every[:, 0:1, :], axis=0)
-    summed = jnp.sum(every[:, 1:2, :] * jnp.exp(every[:, 0:1, :] - peak[None]), axis=0)
-    hit_score = jnp.sum(every[:, 2:3, :], axis=0)
+    maxima = every[:, 0:groups, :]
+    peak = jnp.max(maxima, axis=0)
+    summed = jnp.sum(every[:, groups : 2 * groups, :] * jnp.exp(maxima - peak[None]), axis=0)
+    hit_score = jnp.sum(every[:, 2 * groups : 3 * groups, :], axis=0)
     log_total = peak + jnp.log(summed)
     loss = log_total - hit_score + penalty * log_total * log_total
-    stacked = jnp.concatenate([log_total, loss, jnp.zeros((126, total), f32)], axis=0)
+
+    def one_row(v):
+        return jnp.concatenate([v[c : c + 1, :] for c in range(groups)], axis=1)
+
+    stacked = jnp.concatenate(
+        [one_row(log_total), one_row(loss), jnp.zeros((126, total), f32)], axis=0
+    )
     colv[...] = jnp.transpose(stacked).reshape(n, own_rows, 128)
-    loss_ref[...] = colv[me][:, 1:2]
-
-    def grads(b, _):
+
+    def grads(b):
         lt = colv[b][:, 0:1]
-        w = wgt_ref[b]
-        hit = column_ids == tgt_ref[b] - me * columns
+        w = tw[b][:, 1:2]
+        hit = column_ids == tw[b][:, 0:1]
         probs = jnp.exp(scores[b] - lt)
         sg[b] = (
             w * ((1.0 + 2.0 * penalty * lt) * probs - jnp.where(hit, 1.0, 0.0))
         ).astype(bf16)
-        return 0
-
-    lax.fori_loop(0, n, grads, 0)
-
-    def x_send(slot, j):
-        return pltpu.make_async_remote_copy(
-            src_ref=xsend.at[slot], dst_ref=xrecv.at[slot], send_sem=xs.at[slot], recv_sem=xr.at[slot],
+
+    def lane_part(h):
+        return pl.ds(h * half, half)
+
+    def x_send(slot, j, h):
+        return pltpu.make_async_remote_copy(
+            src_ref=xsend.at[slot, :, lane_part(h)], dst_ref=xrecv.at[slot, :, lane_part(h)],
+            send_sem=xs.at[slot * CHUNKS + h], recv_sem=xr.at[slot * CHUNKS + h],
             device_id={"vp": z * nx + (x + j) % nx}, device_id_type=MESH,
         )
 
@@ -216,13 +238,15 @@
         @pl.when((zz >= 0) & (zz < nz) & ((k > 0) | (i == 0)))
         def _():
             b = zz * nx + (x + j) % nx
+            grads(b)
             p = lax.dot_general(sg[b], mat[...], (((1,), (1,)), ((), ())), preferred_element_type=f32)
 
             @pl.when(j > 0)
             def _():
                 slot = (j - 1) * nz + zz
                 xsend[slot] = p.astype(bf16)
-                x_send(slot, j).start()
+                for h in range(CHUNKS):
+                    x_send(slot, j, h).start()
 
             @pl.when(j == 0)
             def _():
@@ -272,62 +296,65 @@
 
         return 0
 
-    def z_copy(i, zz):
-        return pltpu.make_async_remote_copy(
-            src_ref=zsend.at[zz], dst_ref=zrecv.at[i * nz + zz], send_sem=zs.at[zz],
-            recv_sem=zr.at[i * nz + zz],
+    def z_copy(i, zz, h):
+        return pltpu.make_async_remote_copy(
+            src_ref=zsend.at[zz, :, lane_part(h)], dst_ref=zrecv.at[i * nz + zz, :, lane_part(h)],
+            send_sem=zs.at[zz * CHUNKS + h], recv_sem=zr.at[(i * nz + zz) * CHUNKS + h],
             device_id={"vp": (z + 2 * i - 1) * nx + x}, device_id_type=MESH,
         )
 
-    def add_x(zz):
+    def add_x(zz, h):
         for j in range(1, nx):
             slot = (j - 1) * nz + zz
-            x_send(slot, j).wait_recv()
-            part[zz] += xrecv[slot].astype(f32)
-
-    def add_z(i, zz):
-        z_copy(i, zz).wait_recv()
-        part[zz] += zrecv[i * nz + zz].astype(f32)
+            x_send(slot, j, h).wait_recv()
+            part[zz, :, lane_part(h)] += xrecv[slot, :, lane_part(h)].astype(f32)
+
+    def add_z(i, zz, h):
+        z_copy(i, zz, h).wait_recv()
+        part[zz, :, lane_part(h)] += zrecv[i * nz + zz, :, lane_part(h)].astype(f32)
 
     def chain(k):
-        def one(i, _):
+        def one(i, h):
             zz = z + (2 * i - 1) * k
 
             @pl.when((zz >= 0) & (zz < nz))
             def _():
-                add_x(zz)
+                add_x(zz, h)
 
                 @pl.when(((i == 1) & (z > 0)) | ((i == 0) & (z < nz - 1)))
                 def _():
-                    add_z(i, zz)
-
-                zsend[zz] = part[zz].astype(bf16)
-                z_copy(i, zz).start()
-
-            return 0
-
-        lax.fori_loop(0, 2, one, 0)
+                    add_z(i, zz, h)
+
+                zsend[zz, :, lane_part(h)] = part[zz, :, lane_part(h)].astype(bf16)
+                z_copy(i, zz, h).start()
+
+        for h in range(CHUNKS):
+            lax.fori_loop(0, 2, lambda i, c, h=h: (one(i, h), c)[1], 0)
 
     def chain_at(s, _):
         chain(nz - 1 - s)
         return 0
 
     lax.fori_loop(0, 2 * nz * (nx - 1), row_part, 0)
+    lax.fori_loop(2 * nz * (nx - 1), 2 * nz * nx, row_part, 0)
     lax.fori_loop(0, ny, core_part, 0)
-    lax.fori_loop(2 * nz * (nx - 1), 2 * nz * nx, row_part, 0)
     lax.fori_loop(0, 1, chain_at, 0)
     lax.fori_loop(0, ny, own_part, 0)
     lax.fori_loop(1, nz - 1, chain_at, 0)
 
-    add_x(z)
-
-    @pl.when(z > 0)
-    def _():
-        add_z(1, z)
-
-    @pl.when(z < nz - 1)
-    def _():
-        add_z(0, z)
+    own_col = jnp.concatenate([colv[me], jnp.zeros((128 - own_rows, 128), f32)], axis=0)
+    loss_ref[...] = jnp.transpose(own_col)[1:2, :own_rows]
+
+    for h in range(CHUNKS):
+        add_x(z, h)
+
+        @pl.when(z > 0)
+        def _():
+            add_z(1, z, h)
+
+        @pl.when(z < nz - 1)
+        def _():
+            add_z(0, z, h)
 
     hid = hid_ref[...].astype(f32)
     inverse_rms = lax.rsqrt(jnp.mean(hid * hid, axis=-1, keepdims=True) + epsilon)
@@ -352,16 +379,16 @@
             for j in range(1, nx):
                 x_copy(zz, h, j).wait_send()
 
-        for j in range(1, nx):
-            x_send((j - 1) * nz + zz, j).wait_send()
-
-        @pl.when(zz > z)
-        def _():
-            z_copy(1, zz).wait_send()
-
-        @pl.when(zz < z)
-        def _():
-            z_copy(0, zz).wait_send()
+            for j in range(1, nx):
+                x_send((j - 1) * nz + zz, j, h).wait_send()
+
+            @pl.when(zz > z)
+            def _():
+                z_copy(1, zz, h).wait_send()
+
+            @pl.when(zz < z)
+            def _():
+                z_copy(0, zz, h).wait_send()
 
         return 0
 
@@ -394,7 +421,7 @@
         losses, norm_grad, vocab_grad = pl.pallas_call(
             functools.partial(kernel, n, nx, ny),
             out_shape=(
-                jax.ShapeDtypeStruct((own_rows, 1), f32),
+                jax.ShapeDtypeStruct((1, own_rows), f32),
                 jax.ShapeDtypeStruct(block, f32),
                 jax.ShapeDtypeStruct((out_rows, columns), f32),
             ),
@@ -417,8 +444,9 @@
                 pltpu.VMEM((others, out_rows, columns), bf16),
                 pltpu.VMEM((out_rows, columns), f32),
                 pltpu.VMEM((n, own_rows, 128), f32),
-                pltpu.VMEM((8, total), f32),
-                pltpu.VMEM((n, 8, total), f32),
+                pltpu.VMEM((3 * (total // 128), 128), f32),
+                pltpu.VMEM((n, 3 * (total // 128), 128), f32),
+                pltpu.VMEM((n, own_rows, 128), f32),
                 pltpu.VMEM((n, own_rows, 128), f32),
                 dma,
                 dma((n * CHUNKS,)),
@@ -427,10 +455,10 @@
                 dma((xslots * CHUNKS,)),
                 dma((n,)),
                 dma((n,)),
-                dma((xslots,)),
-                dma((xslots,)),
-                dma((nz,)),
-                dma((2 * nz,)),
+                dma((xslots * CHUNKS,)),
+                dma((xslots * CHUNKS,)),
+                dma((nz * CHUNKS,)),
+                dma((2 * nz * CHUNKS,)),
                 dma((ny,)),
                 dma((ny,)),
                 dma((others,)),
@@ -444,10 +472,10 @@
             norm_gain.reshape(1, width),
             vocab_matrix,
             vocab_bias.reshape(1, columns),
-            targets.reshape(n, own_rows, 1),
-            loss_weight.reshape(n, own_rows, 1),
-        )
-        return losses, norm_grad.reshape(own_rows, 1, width), vocab_grad
+            targets.reshape(1, total),
+            loss_weight.reshape(1, total),
+        )
+        return losses.reshape(own_rows, 1), norm_grad.reshape(own_rows, 1, width), vocab_grad
 
     in_specs = (P("vp", "dp", None), P(), P(None, "vp"), P("vp"), P(None, "dp"), P(None, "dp"))
     out_specs = (P("vp", "dp"), P("vp", "dp", None), P("dp", "vp"))

time: 107 us -> 98.8 us (0.923)
  Pallas kernels: 95 us -> 90.8 us
  local copies, waits for them, and re-layouts: 9.39 us -> 7.09 us
  other arithmetic: 1.4 us -> 0 us
    pallas_call x1, Pallas kernels: 95 us -> 90.8 us  [local(): pl.pallas_call(functools.partial(kernel, n, nx, ny), out_shape=(jax.Shape...]
    reshape x2 -> x0, local copies, waits for them, and re-layouts: 2.03 us -> none  [the longest x1 1.02 us: local(): loss_weight.reshape(n, own_rows, 1)]
    unnamed x2 -> x0, other arithmetic: 1.4 us -> none
where the time goes in v2:
time: 98.8 us; the launch traced here: 98.6 us
  Pallas kernels  90.8 us (92%)
  local copies, waits for them, and re-layouts  7.09 us (7%)
    pallas_call x1, Pallas kernels, local(): pl.pallas_call(functools.partial(kernel, n, nx, ny), out_shape=(jax.Shape...  90.8 us
    unnamed x3, local copies, waits for them, and re-layouts  7.09 us

profile of v2, /device:TPU:0, one launch (start us, length us, event | category | flops | bytes accessed | tf_op | source)
XLA Modules:
  0.0 98.6 jit_solution(16088933347462220598)
XLA Ops:
  0.6 90.8 %shard_map.85 = (f32[1,96]{1,0:T(1,128)}, f32[96,2048]{1,0:T(8,128)}, f32[512,1024]{1,0:T(8,128)}) custom-call(bf16[96,2048]{1,0:T(8,128)(2,1)} %bitcast.8, f32[1,2048]{1,0:T(1,128)} %bitcast.9, bf16[2048,1024]{1,0:T(8,128)(2,1)} %mat_hbm.1, f32[1,1024]{1,0:T(1,128)} %bitcast.10, s32[1,768]{1,0:T(1,128)} %bitcast.11, f32[1,768]{1,0:T(1,128)} %bitcast.12), custom_call_target="tpu_custom_call" | custom-call | tf_op jit(solution)/shard_map/pallas_call | solution.py:421
  91.5 2.8 %copy.9 = f32[96,1,2048]{2,1,0:T(1,128)} copy(f32[96,1,2048]{2,0,1:T(8,128)} %bitcast.7) | data formatting | bytes 1572864
  94.3 1.1 %copy.12 = f32[96,1]{0,1:T(1,128)} copy(f32[96,1]{0,1:T(1,128)} %bitcast.13) | data formatting | bytes 768
  95.4 3.2 %copy.13 = f32[512,1024]{1,0:T(8,128)} copy(f32[512,1024]{1,0:T(8,128)} %get-tuple-element.17) | data formatting | bytes 4194304

commit v3 on v2

--- a/solution.py
+++ b/solution.py
@@ -11,6 +11,7 @@
 penalty = 0.005
 MESH = pl.DeviceIdType.MESH
 CHUNKS = 2
+PIECES = 3
 
 
 def kernel(
@@ -66,57 +67,75 @@
     tw[...] = turned.reshape(n, own_rows, 128)
     pl.semaphore_wait(barrier, n - 1 + ny)
 
+    units = width // 128
+    last = max(1, units * 3 // 16)
+    first = (units - last) // 2
+    starts = (0, first * 128, (units - last) * 128)
+    sizes = (first * 128, (units - last - first) * 128, last * 128)
+    direct, across = (0, 1), 2
+
     def ag_copy(b, h, send_sem, target):
-        piece = rows.at[b, :, pl.ds(h * half, half)]
+        piece = rows.at[b, :, pl.ds(starts[h], sizes[h])]
         return pltpu.make_async_remote_copy(
-            src_ref=piece, dst_ref=piece, send_sem=send_sem, recv_sem=ag_r.at[b * CHUNKS + h],
+            src_ref=piece, dst_ref=piece, send_sem=send_sem, recv_sem=ag_r.at[b * PIECES + h],
             device_id={"vp": target}, device_id_type=MESH,
         )
 
-    def up_copy(zz, h):
-        return ag_copy(zz * nx + x, h, ag_up.at[zz * CHUNKS + h], (z + 1) * nx + x)
-
-    def down_copy(zz, h):
-        return ag_copy(zz * nx + x, h, ag_dn.at[zz * CHUNKS + h], (z - 1) * nx + x)
+    def block_of(zz, j):
+        return zz * nx + (x + j) % nx
+
+    def up_copy(zz, h, j=0):
+        at = (j * nz + zz) * PIECES + h
+        return ag_copy(block_of(zz, j), h, ag_up.at[at], (z + 1) * nx + x)
+
+    def down_copy(zz, h, j=0):
+        at = (j * nz + zz) * PIECES + h
+        return ag_copy(block_of(zz, j), h, ag_dn.at[at], (z - 1) * nx + x)
 
     def x_copy(zz, h, j):
         return ag_copy(
-            zz * nx + x, h, ag_x.at[((j - 1) * nz + zz) * CHUNKS + h], z * nx + (x + j) % nx
+            zz * nx + x, h, ag_x.at[((j - 1) * nz + zz) * PIECES + h], z * nx + (x + j) % nx
         )
 
     def got(b, h):
         ag_copy(b, h, ag_up.at[0], (me + 1) % n).wait_recv()
 
-    def forward(k, h):
+    def forward(k, h, j=0):
         below, above = z - k, z + k
 
-        @pl.when(below >= 0)
-        def _():
-            @pl.when(k > 0)
-            def _():
-                got(below * nx + x, h)
+        def cross(zz):
+            if h != across:
+                for to in range(1, nx):
+                    x_copy(zz, h, to).start()
+
+        @pl.when((k >= 0) & (below >= 0))
+        def _():
+            if j > 0:
+                got(block_of(below, j), h)
+            else:
+                @pl.when(k > 0)
+                def _():
+                    got(block_of(below, j), h)
 
             @pl.when(z < nz - 1)
             def _():
-                up_copy(below, h).start()
+                up_copy(below, h, j).start()
 
             @pl.when((k == 0) & (z > 0))
             def _():
-                down_copy(below, h).start()
-
-            for j in range(1, nx):
-                x_copy(below, h, j).start()
+                down_copy(below, h, j).start()
+
+            cross(below)
 
         @pl.when((k > 0) & (above < nz))
         def _():
-            got(above * nx + x, h)
+            got(block_of(above, j), h)
 
             @pl.when(z > 0)
             def _():
-                down_copy(above, h).start()
-
-            for j in range(1, nx):
-                x_copy(above, h, j).start()
+                down_copy(above, h, j).start()
+
+            cross(above)
 
     lanes = lax.broadcasted_iota(jnp.int32, (own_rows, 128), 1)
     column_ids = lax.broadcasted_iota(jnp.int32, (own_rows, columns), 1).astype(f32)
@@ -131,10 +150,16 @@
         statc[b] = jnp.where(lanes == 0, m, jnp.where(lanes == 1, t, g))
 
     def gather_step(k, _):
-        @pl.when(k < nz)
-        def _():
-            for h in range(CHUNKS):
-                forward(k, h)
+        @pl.when(k == 0)
+        def _():
+            for j in range(1, nx):
+                x_copy(z, across, j).start()
+
+        for j in range(1, nx):
+            forward(k - 1, across, j)
+        for h in direct:
+            forward(k, h)
+        forward(k, across)
 
         @pl.when(k == 0)
         def _():
@@ -150,7 +175,7 @@
             def _():
                 @pl.when(j > 0)
                 def _():
-                    for h in range(CHUNKS):
+                    for h in direct:
                         got(b, h)
 
                 score(b)
@@ -367,18 +392,24 @@
         vout_ref[...] += yrecv[q].astype(f32)
 
     def drain(zz, _):
+        for h, j in [(h, 0) for h in range(PIECES)] + [(across, j) for j in range(1, nx)]:
+            @pl.when((zz <= z) & (z < nz - 1))
+            def _():
+                up_copy(zz, h, j).wait_send()
+
+            @pl.when((zz >= z) & (z > 0))
+            def _():
+                down_copy(zz, h, j).wait_send()
+
+        for j in range(1, nx):
+            for h in direct:
+                x_copy(zz, h, j).wait_send()
+
+            @pl.when(zz == z)
+            def _():
+                x_copy(zz, across, j).wait_send()
+
         for h in range(CHUNKS):
-            @pl.when((zz <= z) & (z < nz - 1))
-            def _():
-                up_copy(zz, h).wait_send()
-
-            @pl.when((zz >= z) & (z > 0))
-            def _():
-                down_copy(zz, h).wait_send()
-
-            for j in range(1, nx):
-                x_copy(zz, h, j).wait_send()
-
             for j in range(1, nx):
                 x_send((j - 1) * nz + zz, j, h).wait_send()
 
@@ -449,10 +480,10 @@
                 pltpu.VMEM((n, own_rows, 128), f32),
                 pltpu.VMEM((n, own_rows, 128), f32),
                 dma,
-                dma((n * CHUNKS,)),
-                dma((nz * CHUNKS,)),
-                dma((nz * CHUNKS,)),
-                dma((xslots * CHUNKS,)),
+                dma((n * PIECES,)),
+                dma((n * PIECES,)),
+                dma((n * PIECES,)),
+                dma((xslots * PIECES,)),
                 dma((n,)),
                 dma((n,)),
                 dma((xslots * CHUNKS,)),

time: 98.8 us -> 98.1 us (level)
  no operation moved by 1% of the time
where the time goes in v3:
time: 98.1 us; the launch traced here: 97.9 us
  Pallas kernels  90.2 us (92%)
  local copies, waits for them, and re-layouts  7.09 us (7%)
    pallas_call x1, Pallas kernels, local(): pl.pallas_call(functools.partial(kernel, n, nx, ny), out_shape=(jax.Shape...  90.2 us
    unnamed x3, local copies, waits for them, and re-layouts  7.09 us

profile of v3, /device:TPU:0, one launch (start us, length us, event | category | flops | bytes accessed | tf_op | source)
XLA Modules:
  0.0 97.9 jit_solution(6577136176542815309)
XLA Ops:
  0.6 90.2 %shard_map.85 = (f32[1,96]{1,0:T(1,128)}, f32[96,2048]{1,0:T(8,128)}, f32[512,1024]{1,0:T(8,128)}) custom-call(bf16[96,2048]{1,0:T(8,128)(2,1)} %bitcast.8, f32[1,2048]{1,0:T(1,128)} %bitcast.9, bf16[2048,1024]{1,0:T(8,128)(2,1)} %mat_hbm.1, f32[1,1024]{1,0:T(1,128)} %bitcast.10, s32[1,768]{1,0:T(1,128)} %bitcast.11, f32[1,768]{1,0:T(1,128)} %bitcast.12), custom_call_target="tpu_custom_call" | custom-call | tf_op jit(solution)/shard_map/pallas_call | solution.py:452
  90.8 2.8 %copy.9 = f32[96,1,2048]{2,1,0:T(1,128)} copy(f32[96,1,2048]{2,0,1:T(8,128)} %bitcast.7) | data formatting | bytes 1572864
  93.7 1.1 %copy.12 = f32[96,1]{0,1:T(1,128)} copy(f32[96,1]{0,1:T(1,128)} %bitcast.13) | data formatting | bytes 768
  94.8 3.2 %copy.13 = f32[512,1024]{1,0:T(8,128)} copy(f32[512,1024]{1,0:T(8,128)} %get-tuple-element.17) | data formatting | bytes 4194304
